TPU v7x, 32 devices: a whole 2x2x4 slice. The times are simulated.
32 devices in a mesh: ep: 16 (over z, x, core), tp: 2 (over y).
Axes of the slice: x: 2, y: 2, z: 4, core: 2. Of those that a mesh axis runs over, the one named last changes fastest.
Arguments:
- tokens: bfloat16 [192, 4096], P('ep', 'tp')
- norm_gain: float32 [4096], P('tp'), may hold values from 0.1 to 1.9
- routes: int32 [192, 6], P('ep'), may hold values from 0 to 15, all different within a row; in each aligned block of 12 rows (0 to 11, 12 to 23, ...) at most 5 rows name the same one
- route_weights: float32 [192, 6], P('ep'), may hold values from 0.05 to 1
- expert_gate: bfloat16 [16, 4096, 1024], P('ep', 'tp'), may hold values from -0.09375 to 0.09375
- expert_up: bfloat16 [16, 4096, 1024], P('ep', 'tp'), may hold values from -0.09375 to 0.09375
- expert_down: bfloat16 [16, 1024, 4096], P('ep', None, 'tp'), may hold values from -0.1875 to 0.1875
- shared_gate: bfloat16 [4096, 1024], P('tp'), may hold values from -0.09375 to 0.09375
- shared_up: bfloat16 [4096, 1024], P('tp'), may hold values from -0.09375 to 0.09375
- shared_down: bfloat16 [1024, 4096], P(None, 'tp'), may hold values from -0.1875 to 0.1875
Outputs:
- mixed: bfloat16 [192, 4096], P('ep', 'tp')
Inputs may be any that keep to these rules, and one draw needn't show every extreme that they name: `routes`: each row names 6 different experts; among the rows of one device no expert is named more than 5 times, and in some devices' rows one expert is named exactly 5 times.
All inputs are finite; a program needn't handle non-finite values.
Results may differ from a plain program's by a relative error of at most 0.0068.
Values may be sent and summed in bfloat16 or wider, within the bound.
A program may use at most 64 MiB of HBM per device.

v0:
```python
import jax
import jax.numpy as jnp
from jax import lax
from jax.sharding import PartitionSpec as P


def block_ranks(route_blocks, n_experts):
    onehot = (route_blocks[..., None] == jnp.arange(n_experts, dtype=jnp.int32)).astype(jnp.int32)
    before = jnp.cumsum(onehot, axis=1) - onehot
    return jnp.sum(before * onehot, axis=-1)


def expert_rows(rows, gate_w, up_w, down_w):
    part_gate = jnp.dot(rows, gate_w, preferred_element_type=jnp.float32)
    part_up = jnp.dot(rows, up_w, preferred_element_type=jnp.float32)
    gate, up = (
        lax.psum_scatter(part_gate, "tp", scatter_dimension=1, tiled=True),
        lax.psum_scatter(part_up, "tp", scatter_dimension=1, tiled=True),
    )
    hidden_part = (jax.nn.silu(gate) * up).astype(jnp.bfloat16)
    result = jnp.dot(
        lax.all_gather(hidden_part, "tp", axis=1, tiled=True),
        down_w,
        preferred_element_type=jnp.float32,
    )
    return result.astype(jnp.bfloat16)


def local(
    tokens,
    norm_gain,
    routes,
    route_weights,
    expert_gate,
    expert_up,
    expert_down,
    shared_gate,
    shared_up,
    shared_down,
):
    tok_rows, part_width = tokens.shape
    picks = routes.shape[1]
    width = part_width * lax.axis_size("tp")
    n_experts = lax.axis_size("ep")
    capacity = max(2, tok_rows * picks // n_experts + 1)
    values = tokens.astype(jnp.float32)
    total = lax.psum(jnp.sum(values * values, axis=1), "tp")
    normed = (values * lax.rsqrt(total / width + 1e-06)[:, None] * norm_gain[None, :]).astype(
        jnp.bfloat16
    )
    scaled = 2.5 * route_weights / jnp.sum(route_weights, axis=1, keepdims=True)
    part_gate = jnp.dot(normed, shared_gate, preferred_element_type=jnp.float32)
    part_up = jnp.dot(normed, shared_up, preferred_element_type=jnp.float32)
    shared_g, shared_u = lax.psum((part_gate, part_up), "tp")
    shared_hidden = (jax.nn.silu(shared_g) * shared_u).astype(jnp.bfloat16)
    shared_out = jnp.dot(shared_hidden, shared_down, preferred_element_type=jnp.float32)
    gate_w, up_w, down_w = (expert_gate[0], expert_up[0], expert_down[0])
    ranks = block_ranks(routes.reshape(1, tok_rows * picks), n_experts).reshape(tok_rows, picks)
    target = routes * capacity + ranks
    slots = jnp.arange(n_experts * capacity, dtype=jnp.int32)
    hits = target[:, :, None] == slots[None, None, :]
    select = jnp.any(hits, axis=1).astype(jnp.bfloat16)
    combine = jnp.sum(jnp.where(hits, scaled[:, :, None], 0.0), axis=1)
    outgoing = jnp.einsum("tj,td->jd", select, normed, preferred_element_type=jnp.float32)
    outgoing = outgoing.astype(jnp.bfloat16).reshape(n_experts, capacity, part_width)
    arrived = lax.all_to_all(outgoing, "ep", split_axis=0, concat_axis=0, tiled=True)
    rows = arrived.reshape(-1, part_width)
    result = expert_rows(rows, gate_w, up_w, down_w).reshape(arrived.shape)
    back = lax.all_to_all(result, "ep", split_axis=0, concat_axis=0, tiled=True)
    back_rows = back.reshape(n_experts * capacity, part_width).astype(jnp.float32)
    routed = jnp.dot(combine, back_rows, precision=lax.Precision.HIGHEST)
    return (shared_out + routed).astype(jnp.bfloat16)


def solution(mesh):
    placed = (
        P("ep", "tp"),
        P("tp"),
        P("ep", None),
        P("ep", None),
        P("ep", "tp", None),
        P("ep", "tp", None),
        P("ep", None, "tp"),
        P("tp", None),
        P("tp", None),
        P(None, "tp"),
    )
    return jax.shard_map(
        local, mesh=mesh, in_specs=placed, out_specs=P("ep", "tp"), check_vma=False
    )
```

profile of v0, /device:TPU:0, one launch (start us, length us, event | category | flops | bytes accessed | tf_op | source)
XLA Modules:
  0.0 105.2 jit_solution(2144665040614947249)
XLA Ops:
  6.5 0.0 reduce-scatter.3.cloned.1.call-start
  6.5 0.8 copy.17
  7.3 0.1 eq.40
  7.4 0.1 fusion.14
  7.5 0.1 reduce_window_sum.11
  7.6 0.2 select_reduce_fusion.1
  7.8 0.1 reshape.113
  7.9 1.0 fusion.10
  8.8 0.1 fusion.13
  8.9 5.9 %psum.21 = f32[12]{0:T(128)S(1)} all-reduce(f32[12]{0:T(128)S(1)} %fusion.10), channel_id=1, replica_groups=mesh['ep'=16,'tp'=2] {'tp'}, use_global_device_ids=true, to_apply=%region_1.0 | all-reduce | flops 12 | bytes 96 | tf_op jit(solution)/shard_map/psum | solution.py:47
  14.9 1.1 %convolution_convert_fusion = bf16[80,2048]{1,0:T(8,128)(2,1)S(1)} fusion(pred[12,80]{1,0:T(8,128)(4,1)S(1)} %fusion.13, bf16[12,2048]{1,0:T(8,128)(2,1)} %param.10, f32[2048]{0:T(1024)} %param.11, f32[12]{0:T(128)S(1)} %add_rsqrt_fusion), kind=kOutput, calls=%fused_computation.6 | convolution fusion | flops 4194304 | bytes 386032 | tf_op jit(solution)/shard_map/tj,td->jd/dot_general | solution.py:64
  16.0 0.1 reshape.114
  16.1 20.5 %all_to_all.10 = bf16[16,5,2048]{2,1,0:T(8,128)(2,1)S(1)} all-to-all(bf16[16,5,2048]{2,1,0:T(8,128)(2,1)S(1)} %reshape.114), channel_id=1, replica_groups=mesh['ep'=16,'tp'=2] {'ep'}, dimensions={0} | all-to-all | bytes 655360 | tf_op jit(solution)/shard_map/all_to_all | solution.py:66
  36.6 0.1 reshape.115
  36.8 0.0 copy-start.1
  36.8 0.0 copy-start.2
  36.8 3.8 %fusion.4 = f32[80,1024]{1,0:T(8,128)} fusion(bf16[80,2048]{1,0:T(8,128)(2,1)S(1)} %reshape.115, bf16[1,2048,1024]{2,1,0:T(8,128)(2,1)} %param.14), kind=kOutput, calls=%fused_computation.4 | convolution fusion | flops 335544320 | bytes 4849664 | tf_op jit(solution)/shard_map/dot_general | solution.py:14
  40.6 0.0 reduce-scatter.3.cloned.1.call-update
  40.6 0.0 reduce-scatter.5.cloned.1.call-start
  40.6 3.8 %fusion.2 = f32[80,1024]{1,0:T(8,128)} fusion(bf16[80,2048]{1,0:T(8,128)(2,1)S(1)} %reshape.115, bf16[1,2048,1024]{2,1,0:T(8,128)(2,1)} %param.15), kind=kOutput, calls=%fused_computation.2 | convolution fusion | flops 335544320 | bytes 4849664 | tf_op jit(solution)/shard_map/dot_general | solution.py:15
  44.4 0.0 reduce-scatter.5.cloned.1.call-update
  44.4 0.0 copy-start.3
  44.5 0.0 all-reduce.3.cloned.1.call-start
  44.5 0.0 copy-done.1
  44.5 0.0 copy-done.2
  44.5 0.0 copy-start
  44.5 3.8 %fusion.19 = f32[12,1024]{1,0:T(8,128)} fusion(bf16[2048,1024]{1,0:T(8,128)(2,1)} %param.18, bf16[12,2048]{1,0:T(8,128)(2,1)S(1)} %copy-done.1, f32[2048]{0:T(1024)S(1)} %copy-done.2, f32[12]{0:T(128)S(1)} %add_rsqrt_fusion), kind=kOutput, calls=%fused_computation.29 | convolution fusion | flops 50429952 | bytes 4300848 | tf_op jit(solution)/shard_map/dot_general | solution.py:53
  48.3 0.0 copy-done
  48.3 1.3 %fusion.21 = f32[12,1024]{1,0:T(8,128)} fusion(bf16[2048,1024]{1,0:T(8,128)(2,1)S(1)} %copy-done, bf16[12,2048]{1,0:T(8,128)(2,1)S(1)} %copy-done.1, f32[2048]{0:T(1024)S(1)} %copy-done.2, f32[12]{0:T(128)S(1)} %add_rsqrt_fusion), kind=kOutput, calls=%fused_computation.30 | convolution fusion | flops 50429952 | bytes 4300848 | tf_op jit(solution)/shard_map/dot_general | solution.py:52
  49.6 0.0 all-reduce.3.cloned.1.call-update
  49.7 0.0 copy-done.3
  49.7 3.1 %reduce-scatter.3.cloned.1.call-done = f32[80,512]{1,0:T(8,128)} async-done(((f32[80,1024]{1,0:T(8,128)}), f32[80,512]{1,0:T(8,128)}) %reduce-scatter.3.cloned.1.call-update) | async-done | bytes 163856 | tf_op jit(solution)/shard_map/reduce_scatter | solution.py:17
  52.8 14.7 %reduce-scatter.5.cloned.1.call-done = f32[80,512]{1,0:T(8,128)} async-done(((f32[80,1024]{1,0:T(8,128)}), f32[80,512]{1,0:T(8,128)}) %reduce-scatter.5.cloned.1.call-update) | async-done | bytes 163856 | tf_op jit(solution)/shard_map/reduce_scatter | solution.py:18
  67.5 1.0 multiply_convert_fusion
  68.6 5.1 %all_gather.3 = bf16[80,1024]{1,0:T(8,128)(2,1)S(1)} all-gather(bf16[80,512]{1,0:T(8,128)(2,1)S(1)} %multiply_convert_fusion), channel_id=1, replica_groups=mesh['ep'=16,'tp'=2] {'tp'}, dimensions={1}, use_global_device_ids=true | all-gather | bytes 245760 | tf_op jit(solution)/shard_map/all_gather | solution.py:22
  73.7 3.1 %fusion.6 = bf16[80,2048]{1,0:T(8,128)(2,1)S(1)} fusion(bf16[80,1024]{1,0:T(8,128)(2,1)S(1)} %all_gather.3, bf16[1,1024,2048]{2,1,0:T(8,128)(2,1)} %param.16), kind=kOutput, calls=%fused_computation.7 | convolution fusion | flops 335708160 | bytes 4685824 | tf_op jit(solution)/shard_map/dot_general | solution.py:21
  76.8 0.9 reshape.116
  77.7 5.6 %all-to-all-start.1 = ((bf16[16,5,2048]{2,1,0:T(8,128)(2,1)}), bf16[16,5,2048]{2,1,0:T(8,128)(2,1)S(1)}, u32[]{:S(2)}, u32[]{:S(2)}) async-start(bf16[16,5,2048]{2,1,0:T(8,128)(2,1)} %reshape.116), calls=%async_computation.3 | async-start | bytes 1048576 | tf_op jit(solution)/shard_map/all_to_all | solution.py:69
  83.3 0.1 copy.19
  83.4 0.1 select_reduce_fusion
  83.5 7.9 %all-reduce.3.cloned.1.call-done = (f32[12,1024]{1,0:T(8,128)}, f32[12,1024]{1,0:T(8,128)}) async-done(((f32[12,1024]{1,0:T(8,128)}, f32[12,1024]{1,0:T(8,128)}), (f32[12,1024]{1,0:T(8,128)}, f32[12,1024]{1,0:T(8,128)})) %all-reduce.3.cloned.1.call-update) | async-done | bytes 98320 | tf_op jit(solution)/shard_map/psum | solution.py:54
  91.5 2.9 %fusion.15 = f32[12,2048]{1,0:T(8,128)S(1)} fusion(bf16[1024,2048]{1,0:T(8,128)(2,1)} %param.19, f32[12,1024]{1,0:T(8,128)} %get-tuple-element.5, f32[12,1024]{1,0:T(8,128)} %get-tuple-element.6), kind=kOutput, calls=%fused_computation.23 | convolution fusion | flops 50405376 | bytes 4390912 | tf_op jit(solution)/shard_map/dot_general | solution.py:56
  94.4 3.2 %all-to-all-done.1 = bf16[16,5,2048]{2,1,0:T(8,128)(2,1)S(1)} async-done(((bf16[16,5,2048]{2,1,0:T(8,128)(2,1)}), bf16[16,5,2048]{2,1,0:T(8,128)(2,1)S(1)}, u32[]{:S(2)}, u32[]{:S(2)}) %all-to-all-start.1) | async-done | bytes 327712 | tf_op jit(solution)/shard_map/all_to_all | solution.py:69
  97.6 0.1 reshape.117
  97.7 0.9 fusion.9
  (4 shorter events, 0.0 us)
Async XLA Ops:
  6.5 46.3 %reduce-scatter.3.cloned.1.call-start = ((), (), s32[]{:S(2)}) async-start(), calls=%async_computation.4 | async-start | bytes 491520 | tf_op jit(solution)/shard_map/reduce_scatter | solution.py:17
  36.8 7.7 %copy-start.1 = (bf16[12,2048]{1,0:T(8,128)(2,1)S(1)}, bf16[12,2048]{1,0:T(8,128)(2,1)}, u32[]{:S(2)}) copy-start(bf16[12,2048]{1,0:T(8,128)(2,1)} %param.10) | copy-start | bytes 147460
  36.8 7.7 %copy-start.2 = (f32[2048]{0:T(1024)S(1)}, f32[2048]{0:T(1024)}, u32[]{:S(2)}) copy-start(f32[2048]{0:T(1024)} %param.11) | copy-start | bytes 24580
  40.6 26.9 %reduce-scatter.5.cloned.1.call-start = ((), (), s32[]{:S(2)}) async-start(), calls=%async_computation.5 | async-start | bytes 491520 | tf_op jit(solution)/shard_map/reduce_scatter | solution.py:18
  44.4 5.2 %copy-start.3 = (f32[12,6]{0,1:T(8,128)S(1)}, f32[12,6]{0,1:T(8,128)}, u32[]{:S(2)}) copy-start(f32[12,6]{0,1:T(8,128)} %param.13) | copy-start | bytes 868
  44.5 47.0 %all-reduce.3.cloned.1.call-start = ((), (), s32[]{:S(2)}) async-start(), calls=%async_computation.6 | async-start | bytes 262144 | tf_op jit(solution)/shard_map/psum | solution.py:54
  44.5 3.8 %copy-start = (bf16[2048,1024]{1,0:T(8,128)(2,1)S(1)}, bf16[2048,1024]{1,0:T(8,128)(2,1)}, u32[]{:S(2)}) copy-start(bf16[2048,1024]{1,0:T(8,128)(2,1)} %param.17) | copy-start | bytes 12582916
  77.7 19.9 %all-to-all-start.1 = ((bf16[16,5,2048]{2,1,0:T(8,128)(2,1)}), bf16[16,5,2048]{2,1,0:T(8,128)(2,1)S(1)}, u32[]{:S(2)}, u32[]{:S(2)}) async-start(bf16[16,5,2048]{2,1,0:T(8,128)(2,1)} %reshape.116), calls=%async_computation.3 | async-start | bytes 1048576 | tf_op jit(solution)/shard_map/all_to_all | solution.py:69
Sparse Core Ops, SparseCore 0:
  40.7 12.0 reduce-scatter.2
  55.0 12.4 reduce-scatter.4
  69.9 21.5 all-reduce.2
where the time goes:
time: 106 us; the launch traced here: 105 us
  blocking collectives  31.5 us (30%)
  waiting for transfers between devices  29 us (27%)
  matrix products  20.7 us (20%)
  between operations  13.2 us (12%)
  starting transfers between devices  5.69 us (5%)
  other arithmetic  2.64 us (2%)
  local copies, waits for them, and re-layouts  2.4 us (2%)
    all_to_all x1, blocking collectives, local(): lax.all_to_all(outgoing, 'ep', split_axis=0, concat_axis=0, tiled=True)  20.5 us
    reduce_scatter x1, waiting for transfers between devices, expert_rows(): lax.psum_scatter(part_up, 'tp', scatter_dimension=1, tiled=True)  14.7 us
    psum x1, waiting for transfers between devices, local(): shared_g, shared_u = lax.psum((part_gate, part_up), 'tp')  7.92 us
    psum x1, blocking collectives, local(): total = lax.psum(jnp.sum(values * values, axis=1), 'tp')  5.9 us
    all_to_all x1, starting transfers between devices, local(): back = lax.all_to_all(result, 'ep', split_axis=0, concat_axis=0, tiled=True)  5.61 us
    all_gather x1, blocking collectives, expert_rows(): lax.all_gather(hidden_part, 'tp', axis=1, tiled=True)  5.11 us
    dot_general x1, matrix products, expert_rows(): part_gate = jnp.dot(rows, gate_w, preferred_element_type=jnp.float32)  3.78 us
    dot_general x1, matrix products, local(): part_up = jnp.dot(normed, shared_up, preferred_element_type=jnp.float32)  3.78 us
  transfers between devices with their start and end apart: 4, of which 4 were waited for; matrix products, arithmetic and copies ran while one was open for 16% of the time, Pallas kernels for 0%

commit v1 on v0

v1 whole, which is shorter than its diff:
```python
import functools

import jax
import jax.numpy as jnp
from jax import lax
from jax.experimental import pallas as pl
from jax.experimental.pallas import tpu as pltpu
from jax.sharding import PartitionSpec as P

MESH = pl.DeviceIdType.MESH
F32 = jnp.float32
BF16 = jnp.bfloat16
LANES = 128
TN = (((0,), (0,)), ((), ()))


def silu_mul(g, u):
    return g / (1.0 + jnp.exp(-g)) * u


def kernel(
    n, tp, cap, chunks, pieces,
    x_ref, gain_ref, routes_ref, rw_ref,
    eg_hbm, eu_hbm, ed_hbm, sg_hbm, su_hbm, sd_hbm,
    out_ref,
    wg, wu, wd, vg, vu, vd,
    packed, outbuf, arrive, retbuf, back,
    rows, mine, psend, precv, sssend, ssrecv, shsend, shrecv, acc, shout,
    wsem, dsend, drecv, rsend, rrecv, tsend, trecv, qsend, qrecv, hsend, hrecv,
):
    me = lax.axis_index("ep")
    my_tp = lax.axis_index("tp")
    toks, width = x_ref.shape
    picks = routes_ref.shape[1]
    ff = wg.shape[1]
    fs = vg.shape[1]
    blocks = width // LANES
    jc = blocks * cap
    n_rows = cap * n
    padded = shout.shape[0]
    cols = ff // chunks

    loads = {}
    slot = 0
    for name, src, dst in (
        ("sg", sg_hbm, vg), ("su", su_hbm, vu), ("sd", sd_hbm, vd),
        ("eg", eg_hbm.at[0], wg), ("eu", eu_hbm.at[0], wu), ("ed", ed_hbm.at[0], wd),
    ):
        depth = dst.shape[0] // pieces
        loads[name] = []
        for i in range(pieces):
            c = pltpu.make_async_copy(
                src.at[pl.ds(i * depth, depth)], dst.at[pl.ds(i * depth, depth)], wsem.at[slot]
            )
            c.start()
            loads[name].append(c)
            slot += 1

    barrier = pltpu.get_barrier_semaphore()
    order = sorted(range(1, n), key=lambda i: -min(i, n - i))
    for i in order:
        pl.semaphore_signal(barrier, inc=1, device_id={"ep": lax.rem(me + i, n)}, device_id_type=MESH)
    for i in range(1, tp):
        pl.semaphore_signal(barrier, inc=1, device_id={"tp": lax.rem(my_tp + i, tp)}, device_id_type=MESH)

    routes = routes_ref[...]
    rw = rw_ref[...]
    scaled = 2.5 * rw / jnp.sum(rw, axis=1, keepdims=True)
    lane_e = lax.broadcasted_iota(jnp.int32, (toks, n), 1)
    named = jnp.zeros((toks, n), F32)
    weight = jnp.zeros((toks, n), F32)
    for k in range(picks):
        hit = routes[:, k : k + 1] == lane_e
        named = named + jnp.where(hit, 1.0, 0.0)
        weight = weight + jnp.where(hit, scaled[:, k : k + 1], 0.0)
    row_i = lax.broadcasted_iota(jnp.int32, (toks, toks), 0)
    col_i = lax.broadcasted_iota(jnp.int32, (toks, toks), 1)
    lower = jnp.where(col_i < row_i, 1.0, 0.0)
    before = jnp.dot(lower, named, preferred_element_type=F32)
    place = jnp.where(named > 0.5, before, -1.0)
    spread_e = lax.broadcasted_iota(jnp.int32, (n, n_rows), 0)
    spread_c = lax.broadcasted_iota(jnp.int32, (n, n_rows), 1)
    spread = jnp.where(lax.rem(spread_c, n) == spread_e, 1.0, 0.0)
    place_x = jnp.dot(place, spread, preferred_element_type=F32)
    slot_x = (lax.broadcasted_iota(jnp.int32, (toks, n_rows), 1) // n).astype(F32)
    taken = place_x == slot_x
    w_hi = weight.astype(BF16).astype(F32)
    w_lo = (weight - w_hi).astype(BF16).astype(F32)
    comb_hi = jnp.where(taken, jnp.dot(w_hi, spread, preferred_element_type=F32), 0.0).astype(BF16)
    comb_lo = jnp.where(taken, jnp.dot(w_lo, spread, preferred_element_type=F32), 0.0).astype(BF16)
    select = jnp.where(taken, 1.0, 0.0).astype(BF16)

    def pack(value, j):
        for s in range(cap):
            packed[pl.ds(j * cap + s, n, stride=jc), :] = value[s * n : (s + 1) * n, :]

    def unpack(j):
        return jnp.concatenate(
            [packed[pl.ds(j * cap + s, n, stride=jc), :] for s in range(cap)], axis=0
        )

    x = x_ref[...]
    for j in range(blocks):
        cut = slice(j * LANES, (j + 1) * LANES)
        pack(lax.dot_general(select, x[:, cut], TN, preferred_element_type=F32), j)
    for p in range(n):
        outbuf[p] = packed[pl.ds(p * jc, jc), :].astype(BF16)

    pl.semaphore_wait(barrier, n - 1 + tp - 1)

    def exchange(src, dst, send, recv):
        copies = []
        for i in order:
            to = lax.rem(me + i, n)
            c = pltpu.make_async_remote_copy(
                src_ref=src.at[to], dst_ref=dst.at[me], send_sem=send.at[to], recv_sem=recv.at[me],
                device_id={"ep": to}, device_id_type=MESH,
            )
            c.start()
            copies.append(c)
        return copies

    def arrived(src, dst, send, recv):
        for i in order[::-1]:
            frm = lax.rem(me + i, n)
            pltpu.make_async_remote_copy(
                src_ref=src.at[frm], dst_ref=dst.at[frm], send_sem=send.at[frm], recv_sem=recv.at[frm],
                device_id={"ep": frm}, device_id_type=MESH,
            ).wait_recv()

    def to_tp(src, dst_of, send_of, recv_of):
        copies = []
        for i in range(1, tp):
            c = pltpu.make_async_remote_copy(
                src_ref=src, dst_ref=dst_of(i - 1), send_sem=send_of(i - 1), recv_sem=recv_of(i - 1),
                device_id={"tp": lax.rem(my_tp + i, tp)}, device_id_type=MESH,
            )
            c.start()
            copies.append(c)
        return copies

    pending = exchange(outbuf, arrive, dsend, drecv)
    arrive[me] = outbuf[me]

    xf = x.astype(F32)
    gain = gain_ref[...]
    xg = (xf * gain).astype(BF16)
    ss_own = jnp.sum(xf * xf, axis=1, keepdims=True)
    shsend[...] = jnp.zeros(shsend.shape, F32)
    shsend[0:toks, 2 * fs : 2 * fs + LANES] = jnp.broadcast_to(ss_own, (toks, LANES))
    for name, w, base in (("sg", vg, 0), ("su", vu, fs)):
        for c in loads[name]:
            c.wait()
        shsend[0:toks, base : base + fs] = jnp.dot(xg, w[...], preferred_element_type=F32)
    shcopies = to_tp(shsend, lambda i: shrecv.at[i], lambda i: hsend.at[i], lambda i: hrecv.at[i])
    pending += shcopies
    for name in ("sd", "eg", "eu", "ed"):
        for c in loads[name]:
            c.wait()
    for c in shcopies:
        c.wait_recv()
    total = shsend[...]
    for i in range(tp - 1):
        total = total + shrecv[i]
    r_own = lax.rsqrt(total[:, 2 * fs : 2 * fs + 1] / (width * tp) + 1e-06)
    sh_hidden = silu_mul(total[:, 0:fs] * r_own, total[:, fs : 2 * fs] * r_own).astype(BF16)
    shout[...] = jnp.dot(sh_hidden, vd[...], preferred_element_type=F32)

    arrived(outbuf, arrive, dsend, drecv)
    for p in range(n):
        packed[pl.ds(p * jc, jc), :] = arrive[p].astype(F32)
    ss = jnp.zeros((n_rows, LANES), F32)
    for j in range(blocks):
        cut = slice(j * LANES, (j + 1) * LANES)
        piece = unpack(j)
        ss = ss + piece * piece
        rows[:, cut] = (piece * gain[:, cut]).astype(BF16)
    sssend[...] = jnp.broadcast_to(jnp.sum(ss, axis=1, keepdims=True), (n_rows, LANES))
    sscopies = to_tp(sssend, lambda i: ssrecv.at[i], lambda i: qsend.at[i], lambda i: qrecv.at[i])
    pending += sscopies
    chunk_copies = []
    for c in range(chunks):
        cut = slice(c * cols, (c + 1) * cols)
        g = jnp.dot(rows[...], wg[:, cut], preferred_element_type=F32)
        u = jnp.dot(rows[...], wu[:, cut], preferred_element_type=F32)
        mine[c, :, 0:cols] = g
        mine[c, :, cols : 2 * cols] = u
        psend[c, :, 0:cols] = g.astype(BF16)
        psend[c, :, cols : 2 * cols] = u.astype(BF16)
        copies = to_tp(
            psend.at[c], lambda i: precv.at[i, c],
            lambda i: tsend.at[i * chunks + c], lambda i: trecv.at[i * chunks + c],
        )
        chunk_copies.append(copies)
        pending += copies
    for c in sscopies:
        c.wait_recv()
    ss_all = sssend[...]
    for i in range(tp - 1):
        ss_all = ss_all + ssrecv[i]
    r = lax.rsqrt(ss_all[:, 0:1] / (width * tp) + 1e-06)
    for c in range(chunks):
        for copy in chunk_copies[c]:
            copy.wait_recv()
        both = mine[c]
        for i in range(tp - 1):
            both = both + precv[i, c].astype(F32)
        hidden = silu_mul(both[:, 0:cols] * r, both[:, cols : 2 * cols] * r).astype(BF16)
        part = jnp.dot(hidden, wd[c * cols : (c + 1) * cols, :], preferred_element_type=F32)
        if c == 0:
            acc[...] = part
        elif c < chunks - 1:
            acc[...] += part
        else:
            for j in range(blocks):
                cut = slice(j * LANES, (j + 1) * LANES)
                pack(acc[:, cut] + part[:, cut], j)
    for p in range(n):
        retbuf[p] = packed[pl.ds(p * jc, jc), :].astype(BF16)
    pending += exchange(retbuf, back, rsend, rrecv)
    back[me] = retbuf[me]
    arrived(retbuf, back, rsend, rrecv)
    for p in range(n):
        packed[pl.ds(p * jc, jc), :] = back[p].astype(F32)
    for j in range(blocks):
        cut = slice(j * LANES, (j + 1) * LANES)
        piece = unpack(j).astype(BF16)
        routed = jnp.dot(comb_hi, piece, preferred_element_type=F32)
        routed = routed + jnp.dot(comb_lo, piece, preferred_element_type=F32)
        out_ref[:, cut] = (shout[0:toks, cut] + routed).astype(BF16)
    for c in pending:
        c.wait_send()


def local(tokens, norm_gain, routes, route_weights, eg, eu, ed, sg, su, sd):
    toks, width = tokens.shape
    picks = routes.shape[1]
    n, tp = lax.axis_size("ep"), lax.axis_size("tp")
    cap = max(2, toks * picks // n + 1)
    ff, fs = eg.shape[2], sg.shape[1]
    chunks, pieces = 4, 4
    jc = width // LANES * cap
    n_rows = n * cap
    padded = -(-toks // 16) * 16
    cols = ff // chunks
    others = max(1, tp - 1)
    vmem = pl.BlockSpec(memory_space=pltpu.VMEM)
    hbm = pl.BlockSpec(memory_space=pl.ANY)
    dma = pltpu.SemaphoreType.DMA
    return pl.pallas_call(
        functools.partial(kernel, n, tp, cap, chunks, pieces),
        out_shape=jax.ShapeDtypeStruct((toks, width), BF16),
        in_specs=[vmem] * 4 + [hbm] * 6,
        out_specs=vmem,
        scratch_shapes=[
            pltpu.VMEM((width, ff), BF16), pltpu.VMEM((width, ff), BF16), pltpu.VMEM((ff, width), BF16),
            pltpu.VMEM((width, fs), BF16), pltpu.VMEM((width, fs), BF16), pltpu.VMEM((fs, width), BF16),
            pltpu.VMEM((n * jc, LANES), F32),
            pltpu.VMEM((n, jc, LANES), BF16), pltpu.VMEM((n, jc, LANES), BF16),
            pltpu.VMEM((n, jc, LANES), BF16), pltpu.VMEM((n, jc, LANES), BF16),
            pltpu.VMEM((n_rows, width), BF16),
            pltpu.VMEM((chunks, n_rows, 2 * cols), F32),
            pltpu.VMEM((chunks, n_rows, 2 * cols), BF16),
            pltpu.VMEM((others, chunks, n_rows, 2 * cols), BF16),
            pltpu.VMEM((n_rows, LANES), F32), pltpu.VMEM((others, n_rows, LANES), F32),
            pltpu.VMEM((padded, 2 * fs + LANES), F32), pltpu.VMEM((others, padded, 2 * fs + LANES), F32),
            pltpu.VMEM((n_rows, width), F32), pltpu.VMEM((padded, width), F32),
            dma((6 * pieces,)),
            dma((n,)), dma((n,)), dma((n,)), dma((n,)),
            dma((others * chunks,)), dma((others * chunks,)),
            dma((others,)), dma((others,)), dma((others,)), dma((others,)),
        ],
        compiler_params=pltpu.CompilerParams(
            collective_id=0, has_side_effects=True, vmem_limit_bytes=60 * 1024 * 1024
        ),
    )(tokens, norm_gain.reshape(1, width), routes, route_weights, eg, eu, ed, sg, su, sd)


def solution(mesh):
    placed = (
        P("ep", "tp"),
        P("tp"),
        P("ep", None),
        P("ep", None),
        P("ep", "tp", None),
        P("ep", "tp", None),
        P("ep", None, "tp"),
        P("tp", None),
        P("tp", None),
        P(None, "tp"),
    )
    return jax.shard_map(
        local, mesh=mesh, in_specs=placed, out_specs=P("ep", "tp"), check_vma=False
    )
```

time: 106 us -> 41.6 us (0.39)
  Pallas kernels: 0 us -> 37.1 us
  blocking collectives: 31.5 us -> 0 us
  waiting for transfers between devices: 29 us -> 0 us
  matrix products: 20.7 us -> 0 us
  between operations: 13.2 us -> 0.01 us
  starting transfers between devices: 5.69 us -> 0 us
  other arithmetic: 2.64 us -> 0 us
  local copies, waits for them, and re-layouts: 2.4 us -> 4.2 us
    pallas_call x0 -> x1, Pallas kernels: none -> 37.1 us  [local(): pl.pallas_call(functools.partial(kernel, n, tp, cap, chunks, pieces), out...]
    dot_general x8 -> x0, matrix products: 20.7 us -> none  [the longest x1 3.78 us: expert_rows(): part_gate = jnp.dot(rows, gate_w, preferred_element_type=jnp.float32)]
    all_to_all x1 -> x0, blocking collectives: 20.5 us -> none  [local(): lax.all_to_all(outgoing, 'ep', split_axis=0, concat_axis=0, tiled=True)]
    reduce_scatter x2 -> x0, waiting for transfers between devices: 17.8 us -> none  [the longest x1 14.7 us: expert_rows(): lax.psum_scatter(part_up, 'tp', scatter_dimension=1, tiled=True)]
    psum x1 -> x0, waiting for transfers between devices: 7.92 us -> none  [local(): shared_g, shared_u = lax.psum((part_gate, part_up), 'tp')]
    psum x1 -> x0, blocking collectives: 5.9 us -> none  [local(): total = lax.psum(jnp.sum(values * values, axis=1), 'tp')]
    all_to_all x1 -> x0, starting transfers between devices: 5.61 us -> none  [local(): back = lax.all_to_all(result, 'ep', split_axis=0, concat_axis=0, tiled=True)]
    all_gather x1 -> x0, blocking collectives: 5.11 us -> none  [expert_rows(): lax.all_gather(hidden_part, 'tp', axis=1, tiled=True)]
  transfers between devices with their start and end apart: 4 -> 0, of which waited for: 4 -> 0; matrix products, arithmetic and copies ran while one was open for 16% -> 0% of each run, Pallas kernels for 0% -> 0%
where the time goes in v1:
time: 41.6 us; the launch traced here: 41.3 us
  Pallas kernels  37.1 us (89%)
  local copies, waits for them, and re-layouts  4.2 us (10%)
    pallas_call x1, Pallas kernels, local(): pl.pallas_call(functools.partial(kernel, n, tp, cap, chunks, pieces), out...  37.1 us
    unnamed x3, local copies, waits for them, and re-layouts  4.2 us

profile of v1, /device:TPU:0, one launch (start us, length us, event | category | flops | bytes accessed | tf_op | source)
XLA Modules:
  0.0 41.3 jit_solution(3183057792921570095)
XLA Ops:
  0.0 1.4 %copy.11.routes_ref = s32[12,6]{1,0:T(8,128)} copy(s32[12,6]{0,1:T(8,128)} %param.12) | data formatting | bytes 576 | tf_op args[2]
  1.4 1.4 %copy.12.rw_ref = f32[12,6]{1,0:T(8,128)} copy(f32[12,6]{0,1:T(8,128)} %param.13) | data formatting | bytes 576 | tf_op args[3]
  2.7 37.1 %shard_map.100 = bf16[12,2048]{1,0:T(8,128)(2,1)} custom-call(bf16[12,2048]{1,0:T(8,128)(2,1)} %x_ref.1, f32[1,2048]{1,0:T(1,128)} %bitcast.1, s32[12,6]{1,0:T(8,128)} %copy.11.routes_ref, f32[12,6]{1,0:T(8,128)} %copy.12.rw_ref, bf16[1,2048,1024]{2,1,0:T(8,128)(2,1)} %eg_hbm.1, bf16[1,2048,1024]{2,1,0:T(8,128)(2,1)} %eu_hbm.1, ...), custom_call_target="tpu_custom_call" | custom-call | tf_op jit(solution)/shard_map/pallas_call | solution.py:250
  39.8 1.5 %copy.14 = bf16[12,2048]{1,0:T(8,128)(2,1)} copy(bf16[12,2048]{1,0:T(8,128)(2,1)} %shard_map.100) | data formatting | bytes 98304

commit v2 on v1

v2 whole, which is shorter than its diff:
```python
import functools

import jax
import jax.numpy as jnp
from jax import lax
from jax.experimental import pallas as pl
from jax.experimental.pallas import tpu as pltpu
from jax.sharding import PartitionSpec as P

MESH = pl.DeviceIdType.MESH
F32 = jnp.float32
BF16 = jnp.bfloat16
LANES = 128
TN = (((0,), (0,)), ((), ()))
SPLIT = True
HILO = True


def silu_mul(g, u):
    return g / (1.0 + jnp.exp(-g)) * u


def kernel(
    n, tp, cap, chunks, pieces,
    x_ref, gain_ref, routes_ref, rw_ref,
    eg_hbm, eu_hbm, ed_hbm, sg_hbm, su_hbm, sd_hbm,
    out_ref,
    wg, wu, wd, vg, vu, vd,
    packed, outbuf, arrive, retbuf, back,
    rows, sssend, ssrecv, shsend, shrecv, acc, shout,
    wsem, dsend, drecv, rsend, rrecv, tsend, trecv, qsend, qrecv, hsend, hrecv,
    *exchanged,
):
    me = lax.axis_index("ep")
    my_tp = lax.axis_index("tp")
    toks, width = x_ref.shape
    picks = routes_ref.shape[0]
    ff = wg.shape[1]
    fs = vg.shape[1]
    blocks = width // LANES
    jc = blocks * cap
    n_rows = cap * n
    mine, psend, precv = exchanged[0::3], exchanged[1::3], exchanged[2::3]
    cols = ff // chunks

    barrier = pltpu.get_barrier_semaphore()
    for i in range(1, n):
        pl.semaphore_signal(barrier, inc=1, device_id={"ep": lax.rem(me + i, n)}, device_id_type=MESH)
    for i in range(1, tp):
        pl.semaphore_signal(barrier, inc=1, device_id={"tp": lax.rem(my_tp + i, tp)}, device_id_type=MESH)

    loads = {}
    slot = 0
    for name, src, dst in (
        ("sg", sg_hbm, vg), ("su", su_hbm, vu), ("sd", sd_hbm, vd),
        ("eg", eg_hbm.at[0], wg), ("eu", eu_hbm.at[0], wu), ("ed", ed_hbm.at[0], wd),
    ):
        depth = dst.shape[0] // pieces
        loads[name] = []
        for i in range(pieces):
            c = pltpu.make_async_copy(
                src.at[pl.ds(i * depth, depth)], dst.at[pl.ds(i * depth, depth)], wsem.at[slot]
            )
            c.start()
            loads[name].append(c)
            slot += 1

    routes = routes_ref[...]
    rw = rw_ref[...]
    scaled = 2.5 * rw / jnp.sum(rw, axis=0, keepdims=True)
    expert = lax.broadcasted_iota(jnp.int32, (n, toks), 0)
    named = jnp.zeros((n, toks), F32)
    weight = jnp.zeros((n, toks), F32)
    for k in range(picks):
        hit = routes[k : k + 1, :] == expert
        named = named + jnp.where(hit, 1.0, 0.0)
        weight = weight + jnp.where(hit, scaled[k : k + 1, :], 0.0)
    row_i = lax.broadcasted_iota(jnp.int32, (toks, toks), 0)
    col_i = lax.broadcasted_iota(jnp.int32, (toks, toks), 1)
    earlier = jnp.where(row_i < col_i, 1.0, 0.0).astype(BF16)
    before = jnp.dot(named.astype(BF16), earlier, preferred_element_type=F32)
    place = jnp.where(named > 0.5, before, -1.0)
    w_hi = weight.astype(BF16).astype(F32)
    w_lo = weight - w_hi

    def by_slot(v):
        return jnp.concatenate([jnp.where(place == s, v, 0.0) for s in range(cap)], axis=0).astype(BF16)

    select, comb_hi, comb_lo = by_slot(1.0), by_slot(w_hi), by_slot(w_lo)

    def pack(value, j, m):
        for s in range(cap):
            packed[pl.ds(j * cap + s, m, stride=jc), :] = value[s * m : (s + 1) * m, :]

    def unpack(j, m):
        return jnp.concatenate(
            [packed[pl.ds(j * cap + s, m, stride=jc), :] for s in range(cap)], axis=0
        )

    x = x_ref[...]
    for j in range(blocks):
        cut = slice(j * LANES, (j + 1) * LANES)
        pack(jnp.dot(select, x[:, cut], preferred_element_type=F32), j, n)
    for p in range(n):
        outbuf[p] = packed[pl.ds(p * jc, jc), :].astype(BF16)

    pl.semaphore_wait(barrier, n - 1 + tp - 1)

    def to_tp(src, dst_of, send_of, recv_of):
        copies = []
        for i in range(1, tp):
            c = pltpu.make_async_remote_copy(
                src_ref=src, dst_ref=dst_of(i - 1), send_sem=send_of(i - 1), recv_sem=recv_of(i - 1),
                device_id={"tp": lax.rem(my_tp + i, tp)}, device_id_type=MESH,
            )
            c.start()
            copies.append(c)
        return copies

    quarter = n // 4
    q, inner = me // quarter, lax.rem(me, quarter)
    half, bit = q // 2, lax.rem(q, 2)
    near = (q, 2 * half + 1 - bit)
    far = (2 * (1 - half) + bit, 2 * (1 - half) + 1 - bit)

    def members(quarters):
        return [qt * quarter + lax.rem(inner + i, quarter) for qt in quarters for i in range(quarter)]

    groups = [members(near)] + [members((f,)) for f in far] if SPLIT else [members(near), members(far)]

    def copy_to(src, dst, send, recv, to):
        return pltpu.make_async_remote_copy(
            src_ref=src.at[to], dst_ref=dst.at[me], send_sem=send.at[to], recv_sem=recv.at[me],
            device_id={"ep": to}, device_id_type=MESH,
        )

    def wait_from(src, dst, send, recv, frm):
        pltpu.make_async_remote_copy(
            src_ref=src.at[frm], dst_ref=dst.at[frm], send_sem=send.at[frm], recv_sem=recv.at[frm],
            device_id={"ep": frm}, device_id_type=MESH,
        ).wait_recv()

    pending = []

    def send_group(g, src, dst, send, recv):
        for i, to in enumerate(groups[g]):
            if g or i:
                c = copy_to(src, dst, send, recv, to)
                c.start()
                pending.append(c)

    def wait_group(g, src, dst, send, recv):
        for i, frm in enumerate(groups[g]):
            if g or i:
                wait_from(src, dst, send, recv, frm)

    for g in range(len(groups)):
        send_group(g, outbuf, arrive, dsend, drecv)
    arrive[me] = outbuf[me]

    xf = x.astype(F32)
    gain = gain_ref[...]
    xg = (xf * gain).astype(BF16)
    ss_own = jnp.sum(xf * xf, axis=1, keepdims=True)
    shsend[...] = jnp.zeros(shsend.shape, F32)
    shsend[0:toks, 2 * fs : 2 * fs + LANES] = jnp.broadcast_to(ss_own, (toks, LANES))
    for name, w, base in (("sg", vg, 0), ("su", vu, fs)):
        for c in loads[name]:
            c.wait()
        shsend[0:toks, base : base + fs] = jnp.dot(xg, w[...], preferred_element_type=F32)
    shcopies = to_tp(shsend, lambda i: shrecv.at[i], lambda i: hsend.at[i], lambda i: hrecv.at[i])
    pending.extend(shcopies)
    def finish_shared():
        for c in loads["sd"]:
            c.wait()
        for c in shcopies:
            c.wait_recv()
        total = shsend[...]
        for i in range(tp - 1):
            total = total + shrecv[i]
        r_own = lax.rsqrt(total[:, 2 * fs : 2 * fs + 1] / (width * tp) + 1e-06)
        sh_hidden = silu_mul(total[:, 0:fs] * r_own, total[:, fs : 2 * fs] * r_own).astype(BF16)
        shout[...] = jnp.dot(sh_hidden, vd[...], preferred_element_type=F32)

    def first_half(g):
        m = len(groups[g])
        count, base = m * cap, starts[g]
        low = -(-count // 16) * 16
        wait_group(g, outbuf, arrive, dsend, drecv)
        for i, p in enumerate(groups[g]):
            packed[pl.ds(i * jc, jc), :] = arrive[p].astype(F32)
        ss = jnp.zeros((count, LANES), F32)
        for j in range(blocks):
            cut = slice(j * LANES, (j + 1) * LANES)
            piece = unpack(j, m)
            ss = ss + piece * piece
            scaled_piece = piece * gain[:, cut]
            hi = scaled_piece.astype(BF16)
            rows[0:count, cut] = hi
            if HILO:
                rows[low : low + count, cut] = (scaled_piece - hi.astype(F32)).astype(BF16)
        sssend[base : base + count] = jnp.broadcast_to(jnp.sum(ss, axis=1, keepdims=True), (count, LANES))
        part = pl.ds(base, count)
        copies = to_tp(
            sssend.at[part], lambda i: ssrecv.at[i, part],
            lambda i: qsend.at[i * len(groups) + g], lambda i: qrecv.at[i * len(groups) + g],
        )
        all_copies = [copies]
        pending.extend(copies)
        taken_rows = rows[0 : 2 * low, :] if HILO else rows[0:count, :]
        for c in range(chunks):
            cut = slice(c * cols, (c + 1) * cols)
            for w, at in ((wg, 0), (wu, cols)):
                v = jnp.dot(taken_rows, w[:, cut], preferred_element_type=F32)
                if HILO:
                    v = v[0:count] + v[low : low + count]
                mine[g][c, :, at : at + cols] = v
                psend[g][c, :, at : at + cols] = v.astype(BF16)
            at_sem = lambda i: (i * len(groups) + g) * chunks + c
            copies = to_tp(
                psend[g].at[c], lambda i: precv[g].at[i, c],
                lambda i: tsend.at[at_sem(i)], lambda i: trecv.at[at_sem(i)],
            )
            all_copies.append(copies)
            pending.extend(copies)
        return all_copies

    def second_half(g, all_copies):
        m = len(groups[g])
        count, base = m * cap, starts[g]
        for c in all_copies[0]:
            c.wait_recv()
        ss_all = sssend[base : base + count, :]
        for i in range(tp - 1):
            ss_all = ss_all + ssrecv[i, base : base + count, :]
        r = lax.rsqrt(ss_all[:, 0:1] / (width * tp) + 1e-06)
        for c in range(chunks):
            for copy in all_copies[1 + c]:
                copy.wait_recv()
            both = mine[g][c]
            for i in range(tp - 1):
                both = both + precv[g][i, c].astype(F32)
            hidden = silu_mul(both[:, 0:cols] * r, both[:, cols : 2 * cols] * r).astype(BF16)
            part = jnp.dot(hidden, wd[c * cols : (c + 1) * cols, :], preferred_element_type=F32)
            if c == 0:
                acc[0:count, :] = part
            elif c < chunks - 1:
                acc[0:count, :] += part
            else:
                for j in range(blocks):
                    cut = slice(j * LANES, (j + 1) * LANES)
                    pack(acc[0:count, cut] + part[:, cut], j, m)
        for i, p in enumerate(groups[g]):
            retbuf[p] = packed[pl.ds(i * jc, jc), :].astype(BF16)
        send_group(g, retbuf, back, rsend, rrecv)

    starts = []
    for g in range(len(groups)):
        starts.append(sum(-(-len(groups[i]) * cap // 8) * 8 for i in range(g)))
    if HILO:
        rows[...] = jnp.zeros(rows.shape, BF16)
    for name in ("eg", "eu"):
        for c in loads[name]:
            c.wait()
    states = [first_half(0)]
    finish_shared()
    for c in loads["ed"]:
        c.wait()
    if len(groups) == 3:
        states.append(first_half(1))
        second_half(0, states[0])
        states.append(first_half(2))
    else:
        states.append(first_half(1))
        second_half(0, states[0])
    back[me] = retbuf[me]
    for g in range(1, len(groups)):
        second_half(g, states[g])
    for g in range(len(groups)):
        wait_group(g, retbuf, back, rsend, rrecv)
    for p in range(n):
        packed[pl.ds(p * jc, jc), :] = back[p].astype(F32)
    for j in range(blocks):
        cut = slice(j * LANES, (j + 1) * LANES)
        piece = unpack(j, n).astype(BF16)
        routed = lax.dot_general(comb_hi, piece, TN, preferred_element_type=F32)
        routed = routed + lax.dot_general(comb_lo, piece, TN, preferred_element_type=F32)
        out_ref[:, cut] = (shout[0:toks, cut] + routed).astype(BF16)
    for c in pending:
        c.wait_send()


def local(tokens, norm_gain, routes, route_weights, eg, eu, ed, sg, su, sd):
    toks, width = tokens.shape
    picks = routes.shape[1]
    n, tp = lax.axis_size("ep"), lax.axis_size("tp")
    cap = max(2, toks * picks // n + 1)
    ff, fs = eg.shape[2], sg.shape[1]
    chunks, pieces = 2, 4
    jc = width // LANES * cap
    n_rows = n * cap
    padded = -(-toks // 16) * 16
    cols = ff // chunks
    others = max(1, tp - 1)
    sizes = [n // 2, n // 4, n // 4] if SPLIT else [n // 2, n // 2]
    exchanged = []
    for m in sizes:
        exchanged += [
            pltpu.VMEM((chunks, m * cap, 2 * cols), F32),
            pltpu.VMEM((chunks, m * cap, 2 * cols), BF16),
            pltpu.VMEM((others, chunks, m * cap, 2 * cols), BF16),
        ]
    vmem = pl.BlockSpec(memory_space=pltpu.VMEM)
    hbm = pl.BlockSpec(memory_space=pl.ANY)
    dma = pltpu.SemaphoreType.DMA
    return pl.pallas_call(
        functools.partial(kernel, n, tp, cap, chunks, pieces),
        out_shape=jax.ShapeDtypeStruct((toks, width), BF16),
        in_specs=[vmem] * 4 + [hbm] * 6,
        out_specs=vmem,
        scratch_shapes=[
            pltpu.VMEM((width, ff), BF16), pltpu.VMEM((width, ff), BF16), pltpu.VMEM((ff, width), BF16),
            pltpu.VMEM((width, fs), BF16), pltpu.VMEM((width, fs), BF16), pltpu.VMEM((fs, width), BF16),
            pltpu.VMEM((n * jc, LANES), F32),
            pltpu.VMEM((n, jc, LANES), BF16), pltpu.VMEM((n, jc, LANES), BF16),
            pltpu.VMEM((n, jc, LANES), BF16), pltpu.VMEM((n, jc, LANES), BF16),
            pltpu.VMEM((2 * n_rows, width), BF16),
            pltpu.VMEM((2 * n_rows, LANES), F32), pltpu.VMEM((others, 2 * n_rows, LANES), F32),
            pltpu.VMEM((padded, 2 * fs + LANES), F32), pltpu.VMEM((others, padded, 2 * fs + LANES), F32),
            pltpu.VMEM((n_rows, width), F32), pltpu.VMEM((padded, width), F32),
            dma((6 * pieces,)),
            dma((n,)), dma((n,)), dma((n,)), dma((n,)),
            dma((others * chunks * len(sizes),)), dma((others * chunks * len(sizes),)),
            dma((others * len(sizes),)), dma((others * len(sizes),)), dma((others,)), dma((others,)),
        ] + exchanged,
        compiler_params=pltpu.CompilerParams(
            collective_id=0, has_side_effects=True, vmem_limit_bytes=60 * 1024 * 1024
        ),
    )(tokens, norm_gain.reshape(1, width), routes.T, route_weights.T, eg, eu, ed, sg, su, sd)


def solution(mesh):
    placed = (
        P("ep", "tp"),
        P("tp"),
        P("ep", None),
        P("ep", None),
        P("ep", "tp", None),
        P("ep", "tp", None),
        P("ep", None, "tp"),
        P("tp", None),
        P("tp", None),
        P(None, "tp"),
    )
    return jax.shard_map(
        local, mesh=mesh, in_specs=placed, out_specs=P("ep", "tp"), check_vma=False
    )
```

time: 41.6 us -> 33.4 us (0.80)
  Pallas kernels: 37.1 us -> 31.7 us
  local copies, waits for them, and re-layouts: 4.2 us -> 1.47 us
    pallas_call x1, Pallas kernels: 37.1 us -> 31.7 us  [local(): pl.pallas_call(functools.partial(kernel, n, tp, cap, chunks, pieces), out...]
    unnamed x3 -> x1, local copies, waits for them, and re-layouts: 4.2 us -> 1.47 us
where the time goes in v2:
time: 33.4 us; the launch traced here: 33.2 us
  Pallas kernels  31.7 us (95%)
  local copies, waits for them, and re-layouts  1.47 us (4%)
    pallas_call x1, Pallas kernels, local(): pl.pallas_call(functools.partial(kernel, n, tp, cap, chunks, pieces), out...  31.7 us
    unnamed x1, local copies, waits for them, and re-layouts  1.47 us

profile of v2, /device:TPU:0, one launch (start us, length us, event | category | flops | bytes accessed | tf_op | source)
XLA Modules:
  0.0 33.2 jit_solution(8828738656699796394)
XLA Ops:
  0.0 31.7 %shard_map.100 = bf16[12,2048]{1,0:T(8,128)(2,1)} custom-call(bf16[12,2048]{1,0:T(8,128)(2,1)} %x_ref.1, f32[1,2048]{1,0:T(1,128)} %bitcast.3, s32[6,12]{1,0:T(8,128)} %bitcast.4, f32[6,12]{1,0:T(8,128)} %bitcast.5, bf16[1,2048,1024]{2,1,0:T(8,128)(2,1)} %eg_hbm.1, bf16[1,2048,1024]{2,1,0:T(8,128)(2,1)} %eu_hbm.1, bf16[1,1024,2048]{2,1,0:T(8,128)(2,1)} %ed_hbm.1, ...), custom_call_target="tpu_custom_call" | custom-call | tf_op jit(solution)/shard_map/pallas_call | solution.py:316
  31.7 1.5 %copy.12 = bf16[12,2048]{1,0:T(8,128)(2,1)} copy(bf16[12,2048]{1,0:T(8,128)(2,1)} %shard_map.100) | data formatting | bytes 98304
